TPU v7x, 32 devices: a whole 2x2x4 slice. The times are simulated.
32 devices in a mesh: fs: 16 (over z, y, x), tp: 2 (over core).
Axes of the slice: x: 2, y: 2, z: 4, core: 2. Of those that a mesh axis runs over, the one named last changes fastest.
Arguments:
- tokens: bfloat16 [2048, 2048], P('fs', 'tp'), may hold values from -300 to 300
- norm_gain: float32 [2048], P('fs'), may hold values from 0.1 to 1.9
- gate_weight: float32 [16, 2048, 1024], P(None, 'fs', 'tp'), may hold values from -1.3258252 to 1.3258252
- up_weight: float32 [16, 2048, 1024], P(None, 'fs', 'tp'), may hold values from -1.3258252 to 1.3258252
- down_weight: float32 [16, 1024, 2048], P(None, 'fs', 'tp'), may hold values from -0.1875 to 0.1875
- routes: int32 [2048, 4], P('fs'), may hold values from 0 to 15, all different within a row; in each aligned block of 128 rows (0 to 127, 128 to 255, ...) at most 64 rows name the same one
- route_weights: float32 [2048, 4], P('fs'), may hold values from 0.05 to 1
Outputs:
- mixed: bfloat16 [2048, 2048], P('fs', 'tp')
- gate_ready: bfloat16 [16, 2048, 1024], P('fs', None, 'tp')
- up_ready: bfloat16 [16, 2048, 1024], P('fs', None, 'tp')
- down_ready: bfloat16 [16, 1024, 2048], P('fs', None, 'tp')
Inputs may be any that keep to these rules, and one draw needn't show every extreme that they name: `routes`: each row names 4 different experts. In each aligned block of 128 rows no expert is named more than 64 times, a bound that some block reaches.
All inputs are finite; a program needn't handle non-finite values.
Results may differ from a plain program's by a relative error of at most 0.0089.
Values may be sent and summed in bfloat16 or wider, within the bound.
A program may use at most 64 MiB of HBM per device.

v0:
```python
import jax
import jax.numpy as jnp
from jax import lax
from jax.sharding import PartitionSpec as P

epsilon = 1e-05


def activate(gate_pre, up_pre):
    gated = jnp.minimum(gate_pre, 7.0)
    upper = jnp.clip(up_pre, -7.0, 7.0)
    return (upper + 1.0) * gated * jax.nn.sigmoid(1.702 * gated)


def shards(tokens, norm_gain, gate_weight, up_weight, down_weight, routes, route_weights):
    gate_send = (norm_gain[None, :, None] * gate_weight).astype(jnp.bfloat16)
    up_send = (norm_gain[None, :, None] * up_weight).astype(jnp.bfloat16)
    down_send = down_weight.astype(jnp.bfloat16)
    gate_ready, up_ready, down_ready = (
        lax.all_to_all(gate_send, "fs", split_axis=0, concat_axis=1, tiled=True),
        lax.all_to_all(up_send, "fs", split_axis=0, concat_axis=1, tiled=True),
        lax.all_to_all(down_send, "fs", split_axis=0, concat_axis=1, tiled=True),
    )
    experts = gate_weight.shape[0]
    tok_rows = tokens.shape[0]
    top_count = routes.shape[1]
    pairs = tok_rows * top_count
    capacity = 2 * pairs // experts
    chosen = routes.reshape(pairs)
    onehot = (chosen[:, None] == jnp.arange(experts, dtype=jnp.int32)[None, :]).astype(jnp.int32)
    position = jnp.sum(jnp.cumsum(onehot, axis=0) * onehot, axis=1) - 1
    slot_index = chosen * capacity + position
    token_index = jnp.arange(pairs, dtype=jnp.int32) // top_count
    values = tokens.astype(jnp.float32)
    squared = lax.psum(jnp.sum(values * values, axis=1), "tp")
    width = values.shape[1] * lax.axis_size("tp")
    normed = (values * lax.rsqrt(squared / width + epsilon)[:, None]).astype(jnp.bfloat16)
    outbound = jnp.zeros((experts * capacity, normed.shape[1]), jnp.bfloat16)
    outbound = (
        outbound.at[slot_index].set(normed[token_index]).reshape(experts, capacity, normed.shape[1])
    )
    gate_matrix = gate_ready[0]
    up_matrix = up_ready[0]
    down_matrix = down_ready[0]
    arrived = lax.all_to_all(outbound, "fs", split_axis=0, concat_axis=0, tiled=True)
    arrived = lax.all_gather(arrived, "tp", axis=2, tiled=True)
    sources = arrived.shape[0]
    items = arrived.shape[1]
    arrived_rows = arrived.reshape(sources * items, arrived.shape[2])
    gate_pre = jnp.dot(arrived_rows, gate_matrix, preferred_element_type=jnp.float32)
    up_pre = jnp.dot(arrived_rows, up_matrix, preferred_element_type=jnp.float32)
    hidden = activate(gate_pre, up_pre).astype(jnp.bfloat16)
    summed = jnp.dot(
        lax.all_gather(hidden, "tp", axis=1, tiled=True),
        down_matrix,
        preferred_element_type=jnp.float32,
    )
    results = summed.astype(jnp.bfloat16).reshape(sources, items, down_matrix.shape[1])
    returned = lax.all_to_all(results, "fs", split_axis=0, concat_axis=0, tiled=True)
    flat_back = returned.reshape(experts * capacity, returned.shape[2])
    picked = (
        flat_back[slot_index].astype(jnp.float32).reshape(tok_rows, top_count, returned.shape[2])
    )
    mixed = jnp.sum(picked * route_weights[:, :, None], axis=1).astype(jnp.bfloat16)
    return (mixed, gate_ready, up_ready, down_ready)


def solution(mesh):
    placed = (
        P("fs", "tp"),
        P("fs"),
        P(None, "fs", "tp"),
        P(None, "fs", "tp"),
        P(None, "fs", "tp"),
        P("fs", None),
        P("fs", None),
    )
    return jax.shard_map(
        shards,
        mesh=mesh,
        in_specs=placed,
        out_specs=(P("fs", "tp"), P("fs", None, "tp"), P("fs", None, "tp"), P("fs", None, "tp")),
        check_vma=False,
    )
```

profile of v0, /device:TPU:20, one launch (start us, length us, event | category | flops | bytes accessed | tf_op | source)
XLA Modules:
  0.0 311.5 jit_solution(14182321171666740326)
XLA Ops:
  7.2 0.8 copy.13
  8.2 0.7 broadcast_multiply_fusion
  8.9 1.2 reduce-window.6
  10.0 0.2 slice_reduce_fusion
  10.4 0.1 copy.12
  10.6 1.1 fusion.3
  11.7 2.5 psum.7
  14.2 1.1 fusion.4
  15.3 7.7 %scatter_custom_fusion = bf16[1024,1024]{1,0:T(8,128)(2,1)} fusion(s32[512]{0:T(512)S(1)} %bitcast.38, bf16[128,1024]{1,0:T(8,128)(2,1)S(1)} %fusion.4, s32[1024]{0:T(1024)S(1)} %pad_clamp_fusion.1, bf16[]{:T(256)} %constant.15.clone.1), kind=kCustom, calls=%fused_computation.8 | custom fusion | bytes 2097154 | tf_op jit(solution)/shard_map/scatter | solution.py:40
  23.0 7.2 %all-to-all-start = ((bf16[16,64,1024]{2,1,0:T(8,128)(2,1)}), bf16[16,64,1024]{2,1,0:T(8,128)(2,1)}, u32[]{:S(2)}, u32[]{:S(2)}) async-start(bf16[16,64,1024]{2,1,0:T(8,128)(2,1)} %bitcast.4), calls=%async_computation | async-start | bytes 4194304 | tf_op jit(solution)/shard_map/all_to_all | solution.py:45
  30.2 6.1 %multiply_convert_fusion = (bf16[16,128,512]{2,1,0:T(8,128)(2,1)}, bf16[16,128,512]{2,1,0:T(8,128)(2,1)S(1)}) fusion(f32[16,128,512]{2,1,0:T(8,128)} %param.9, f32[128]{0:T(128)S(1)} %copy-done.3, f32[16,128,512]{2,1,0:T(8,128)} %param.10), kind=kLoop, calls=%fused_computation.3 | loop fusion | flops 4194304 | bytes 12583424 | tf_op jit(solution)/shard_map/convert_element_type | solution.py:16
  36.3 40.4 %all-to-all-done = bf16[16,64,1024]{2,1,0:T(8,128)(2,1)} async-done(((bf16[16,64,1024]{2,1,0:T(8,128)(2,1)}), bf16[16,64,1024]{2,1,0:T(8,128)(2,1)}, u32[]{:S(2)}, u32[]{:S(2)}) %all-to-all-start) | async-done | bytes 2097184 | tf_op jit(solution)/shard_map/all_to_all | solution.py:45
  76.7 52.4 %all_to_all.46 = bf16[16,128,512]{2,1,0:T(8,128)(2,1)} all-to-all(bf16[16,128,512]{2,1,0:T(8,128)(2,1)S(1)} %get-tuple-element.5), channel_id=1, replica_groups=mesh['fs'=16,'tp'=2] {'fs'}, dimensions={0} | all-to-all | bytes 4194304 | tf_op jit(solution)/shard_map/all_to_all | solution.py:21
  129.2 7.0 %all-to-all-start.2 = ((bf16[16,128,512]{2,1,0:T(8,128)(2,1)}), bf16[16,128,512]{2,1,0:T(8,128)(2,1)}, u32[]{:S(2)}, u32[]{:S(2)}) async-start(bf16[16,128,512]{2,1,0:T(8,128)(2,1)} %get-tuple-element.4), calls=%async_computation.2 | async-start | bytes 4194304 | tf_op jit(solution)/shard_map/all_to_all | solution.py:20
  136.2 0.7 all-gather.3.cloned.1.call-update
  136.9 3.8 %convert_element_type.42 = bf16[16,64,1024]{2,1,0:T(8,128)(2,1)} convert(f32[16,64,1024]{2,1,0:T(8,128)} %param.11) | non-fusion elementwise | flops 1048576 | bytes 6291456 | tf_op jit(solution)/shard_map/convert_element_type | solution.py:18
  140.7 40.5 %all-to-all-done.2 = bf16[16,128,512]{2,1,0:T(8,128)(2,1)} async-done(((bf16[16,128,512]{2,1,0:T(8,128)(2,1)}), bf16[16,128,512]{2,1,0:T(8,128)(2,1)}, u32[]{:S(2)}, u32[]{:S(2)}) %all-to-all-start.2) | async-done | bytes 2097184 | tf_op jit(solution)/shard_map/all_to_all | solution.py:20
  181.3 7.0 %all-to-all-start.3 = ((bf16[16,64,1024]{2,1,0:T(8,128)(2,1)}), bf16[16,64,1024]{2,1,0:T(8,128)(2,1)}, u32[]{:S(2)}, u32[]{:S(2)}) async-start(bf16[16,64,1024]{2,1,0:T(8,128)(2,1)} %convert_element_type.42), calls=%async_computation.3 | async-start | bytes 4194304 | tf_op jit(solution)/shard_map/all_to_all | solution.py:22
  188.3 0.2 all-gather.5.cloned.1.call-start
  188.6 4.7 %fusion.8 = f32[1024,512]{1,0:T(8,128)S(1)} fusion(bf16[1024,2048]{1,0:T(8,128)(2,1)} %bitcast.42, bf16[2048,512]{1,0:T(8,128)(2,1)S(1)} %bitcast.35), kind=kOutput, calls=%fused_computation.34 | convolution fusion | flops 2147483648 | bytes 8388608 | tf_op jit(solution)/shard_map/dot_general | solution.py:51
  193.2 5.4 %multiply_convert_fusion.2 = bf16[1024,512]{1,0:T(8,128)(2,1)} fusion(f32[1024,512]{1,0:T(8,128)S(1)} %fusion.8, bf16[1024,2048]{1,0:T(8,128)(2,1)S(1)} %bitcast.43, bf16[2048,512]{1,0:T(8,128)(2,1)} %bitcast.7), kind=kOutput, calls=%fused_computation.6 | convolution fusion | flops 2152726528 | bytes 9437184 | tf_op jit(solution)/shard_map/dot_general | solution.py:50
  198.7 35.1 %all-to-all-done.3 = bf16[16,64,1024]{2,1,0:T(8,128)(2,1)} async-done(((bf16[16,64,1024]{2,1,0:T(8,128)(2,1)}), bf16[16,64,1024]{2,1,0:T(8,128)(2,1)}, u32[]{:S(2)}, u32[]{:S(2)}) %all-to-all-start.3) | async-done | bytes 2097184 | tf_op jit(solution)/shard_map/all_to_all | solution.py:22
  233.7 5.9 %convolution_convert_fusion = bf16[1024,1024]{1,0:T(8,128)(2,1)} fusion(bf16[1024,1024]{1,0:T(8,128)(2,1)} %all-gather.5.cloned.1.call-done, bf16[1024,1024]{1,0:T(8,128)(2,1)} %bitcast.8), kind=kOutput, calls=%fused_computation.7 | convolution fusion | flops 2148532224 | bytes 6291456 | tf_op jit(solution)/shard_map/dot_general | solution.py:53
  239.6 7.2 %all-to-all-start.4 = ((bf16[16,64,1024]{2,1,0:T(8,128)(2,1)}), bf16[16,64,1024]{2,1,0:T(8,128)(2,1)S(1)}, u32[]{:S(2)}, u32[]{:S(2)}) async-start(bf16[16,64,1024]{2,1,0:T(8,128)(2,1)} %bitcast.37), calls=%async_computation.4 | async-start | bytes 4194304 | tf_op jit(solution)/shard_map/all_to_all | solution.py:59
  246.8 0.1 copy.16
  246.9 45.3 %all-to-all-done.4 = bf16[16,64,1024]{2,1,0:T(8,128)(2,1)S(1)} async-done(((bf16[16,64,1024]{2,1,0:T(8,128)(2,1)}), bf16[16,64,1024]{2,1,0:T(8,128)(2,1)S(1)}, u32[]{:S(2)}, u32[]{:S(2)}) %all-to-all-start.4) | async-done | bytes 2097184 | tf_op jit(solution)/shard_map/all_to_all | solution.py:59
  292.2 2.0 gather_fusion
  294.3 0.7 reshape.141
  295.0 2.1 multiply_reduce_fusion
  297.1 3.2 %copy.22 = bf16[1,2048,512]{2,1,0:T(8,128)(2,1)} copy(bf16[1,2048,512]{2,1,0:T(8,128)(2,1)} %bitcast.11) | data formatting | bytes 4194304
  300.3 1.3 copy.23
  301.6 3.1 copy.24
  (27 shorter events, 0.6 us)
Async XLA Ops:
  23.0 7.2 %copy-start.3 = (f32[128]{0:T(128)S(1)}, f32[128]{0:T(128)}, u32[]{:S(2)}) copy-start(f32[128]{0:T(128)} %param.8) | copy-start | bytes 1540
  23.0 53.7 %all-to-all-start = ((bf16[16,64,1024]{2,1,0:T(8,128)(2,1)}), bf16[16,64,1024]{2,1,0:T(8,128)(2,1)}, u32[]{:S(2)}, u32[]{:S(2)}) async-start(bf16[16,64,1024]{2,1,0:T(8,128)(2,1)} %bitcast.4), calls=%async_computation | async-start | bytes 4194304 | tf_op jit(solution)/shard_map/all_to_all | solution.py:45
  129.2 52.1 %all-to-all-start.2 = ((bf16[16,128,512]{2,1,0:T(8,128)(2,1)}), bf16[16,128,512]{2,1,0:T(8,128)(2,1)}, u32[]{:S(2)}, u32[]{:S(2)}) async-start(bf16[16,128,512]{2,1,0:T(8,128)(2,1)} %get-tuple-element.4), calls=%async_computation.2 | async-start | bytes 4194304 | tf_op jit(solution)/shard_map/all_to_all | solution.py:20
  136.1 52.4 %all-gather.3.cloned.1.call-start = ((), (), s32[]{:S(2)}) async-start(), calls=%async_computation.5 | async-start | bytes 6291456 | tf_op jit(solution)/shard_map/all_gather | solution.py:46
  140.7 47.8 %copy-start = (bf16[16,128,512]{2,1,0:T(8,128)(2,1)S(1)}, bf16[16,128,512]{2,1,0:T(8,128)(2,1)}, u32[]{:S(2)}) copy-start(bf16[16,128,512]{2,1,0:T(8,128)(2,1)} %all_to_all.46) | copy-start | bytes 6291460
  181.3 52.5 %all-to-all-start.3 = ((bf16[16,64,1024]{2,1,0:T(8,128)(2,1)}), bf16[16,64,1024]{2,1,0:T(8,128)(2,1)}, u32[]{:S(2)}, u32[]{:S(2)}) async-start(bf16[16,64,1024]{2,1,0:T(8,128)(2,1)} %convert_element_type.42), calls=%async_computation.3 | async-start | bytes 4194304 | tf_op jit(solution)/shard_map/all_to_all | solution.py:22
  188.3 45.4 %all-gather.5.cloned.1.call-start = ((), (), s32[]{:S(2)}) async-start(), calls=%async_computation.6 | async-start | bytes 3145728 | tf_op jit(solution)/shard_map/all_gather | solution.py:54
  188.6 4.7 %copy-start.4 = (bf16[16,64,2048]{2,1,0:T(8,128)(2,1)S(1)}, bf16[16,64,2048]{2,1,0:T(8,128)(2,1)}, u32[]{:S(2)}) copy-start(bf16[16,64,2048]{2,1,0:T(8,128)(2,1)} %all-gather.3.cloned.1.call-done) | copy-start | bytes 12582916
  239.6 7.2 %copy-start.2 = (f32[128,4]{0,1:T(4,128)S(1)}, f32[128,4]{0,1:T(4,128)}, u32[]{:S(2)}) copy-start(f32[128,4]{0,1:T(4,128)} %param.13) | copy-start | bytes 6148
  239.6 52.6 %all-to-all-start.4 = ((bf16[16,64,1024]{2,1,0:T(8,128)(2,1)}), bf16[16,64,1024]{2,1,0:T(8,128)(2,1)S(1)}, u32[]{:S(2)}, u32[]{:S(2)}) async-start(bf16[16,64,1024]{2,1,0:T(8,128)(2,1)} %bitcast.37), calls=%async_computation.4 | async-start | bytes 4194304 | tf_op jit(solution)/shard_map/all_to_all | solution.py:59
  297.1 3.2 %copy-start.1 = (bf16[16,128,512]{2,1,0:T(8,128)(2,1)S(1)}, bf16[16,128,512]{2,1,0:T(8,128)(2,1)}, u32[]{:S(2)}) copy-start(bf16[16,128,512]{2,1,0:T(8,128)(2,1)} %all_to_all.46) | copy-start | bytes 6291460
Sparse Core Ops, SparseCore 0:
  138.5 14.8 all-gather.2
  198.8 11.7 all-gather.4
where the time goes:
time: 314 us; the launch traced here: 312 us
  waiting for transfers between devices  162 us (52%)
  blocking collectives  54.9 us (17%)
  starting transfers between devices  28.6 us (9%)
  local copies, waits for them, and re-layouts  19.6 us (6%)
  other arithmetic  16.2 us (5%)
  matrix products  15.9 us (5%)
  between operations  14.2 us (5%)
    all_to_all x1, blocking collectives, shards(): lax.all_to_all(up_send, 'fs', split_axis=0, concat_axis=1, tiled=True)  52.4 us
    all_to_all x1, waiting for transfers between devices, shards(): lax.all_to_all(results, 'fs', split_axis=0, concat_axis=0, tiled=True)  45.3 us
    all_to_all x1, waiting for transfers between devices, shards(): lax.all_to_all(gate_send, 'fs', split_axis=0, concat_axis=1, tiled=True)  40.5 us
    all_to_all x1, waiting for transfers between devices, shards(): lax.all_to_all(outbound, 'fs', split_axis=0, concat_axis=0, tiled=True)  40.4 us
    all_to_all x1, waiting for transfers between devices, shards(): lax.all_to_all(down_send, 'fs', split_axis=0, concat_axis=1, tiled=True)  35.1 us
    unnamed x15, local copies, waits for them, and re-layouts  8.51 us
    scatter x1, local copies, waits for them, and re-layouts, shards(): outbound.at[slot_index].set(normed[token_index])  7.72 us
    all_to_all x1, starting transfers between devices, shards(): lax.all_to_all(outbound, 'fs', split_axis=0, concat_axis=0, tiled=True)  7.19 us
  transfers between devices with their start and end apart: 6, of which 4 were waited for; matrix products, arithmetic and copies ran while one was open for 6% of the time, Pallas kernels for 0%

commit v1 on v0

v1 whole, which is shorter than its diff:
```python
import functools

import jax
import jax.numpy as jnp
from jax import lax
from jax.experimental import pallas as pl
from jax.experimental.pallas import tpu as pltpu
from jax.sharding import PartitionSpec as P

epsilon = 1e-05
MESH = pl.DeviceIdType.MESH
GROUPS = 4


def activate(gate_pre, up_pre):
    gated = jnp.minimum(gate_pre, 7.0)
    upper = jnp.clip(up_pre, -7.0, 7.0)
    return (upper + 1.0) * gated * jax.nn.sigmoid(1.702 * gated)


def kernel(
    n, cores, slots_in, gate_in, up_in, down_in, mix_high, mix_low,
    mixed_out, gate_out, up_out, down_out,
    rows, gate, up, down, hidden, results, back,
    send_sem, recv_sem, own_sem, out_sem, tp_send, tp_recv,
):
    me = lax.axis_index("fs")
    core = lax.axis_index("tp")
    depth = gate_in.shape[1]
    units = down_in.shape[1]
    items = slots_in.shape[1]
    total = n * items
    width = slots_in.shape[2]
    columns = gate_in.shape[2]

    barrier = pltpu.get_barrier_semaphore()

    def greet(step, carry):
        pl.semaphore_signal(barrier, inc=1, device_id={"fs": lax.rem(me + step, n)}, device_id_type=MESH)
        return carry

    lax.fori_loop(1, n, greet, 0)
    for step in range(1, cores):
        pl.semaphore_signal(barrier, inc=1, device_id={"tp": lax.rem(core + step, cores)}, device_id_type=MESH)
    pl.semaphore_wait(barrier, n - 1 + cores - 1)

    mine = rows.at[core]
    phases = ((slots_in, mine, items), (gate_in, gate, depth), (up_in, up, depth), (down_in, down, units))

    def own(phase):
        source, landing, size = phases[phase]
        return pltpu.make_async_copy(source.at[me], landing.at[pl.ds(me * size, size)], own_sem.at[phase])

    def start(phase):
        source, landing, size = phases[phase]

        def send(step, carry):
            peer = lax.rem(me + step, n)
            pltpu.make_async_remote_copy(
                src_ref=source.at[peer],
                dst_ref=landing.at[pl.ds(me * size, size)],
                send_sem=send_sem.at[phase],
                recv_sem=recv_sem.at[phase],
                device_id={"fs": peer},
                device_id_type=MESH,
            ).start()
            return carry

        own(phase).start()
        lax.fori_loop(1, n, send, 0)

    def drain(landing, size, semaphore):
        piece = landing.at[pl.ds(0, (n - 1) * size)]
        pltpu.make_async_copy(piece, piece, semaphore).wait()

    def arrive(phase):
        _, landing, size = phases[phase]
        drain(landing, size, recv_sem.at[phase])
        own(phase).wait()

    def swap(buffer, slot):
        copies = []
        for step in range(1, cores):
            copies.append(
                pltpu.make_async_remote_copy(
                    src_ref=buffer.at[core],
                    dst_ref=buffer.at[core],
                    send_sem=tp_send.at[slot, step - 1],
                    recv_sem=tp_recv.at[slot, step - 1],
                    device_id={"tp": lax.rem(core + step, cores)},
                    device_id_type=MESH,
                )
            )
        for copy in copies:
            copy.start()
        return copies

    for phase in range(4):
        start(phase)

    arrive(0)
    swapped = swap(rows, 0)
    arrive(1)
    gate_copy = pltpu.make_async_copy(gate, gate_out, out_sem.at[0])
    gate_copy.start()
    for copy in swapped:
        copy.wait()
    arrive(2)
    up_copy = pltpu.make_async_copy(up, up_out, out_sem.at[1])
    up_copy.start()

    tile = total // GROUPS

    def first_layer(group, carry):
        at = pl.ds(pl.multiple_of(group * tile, tile), tile)
        gate_pre = jnp.zeros((tile, columns), jnp.float32)
        up_pre = jnp.zeros((tile, columns), jnp.float32)
        for part in range(cores):
            block = rows[part, at, :]
            span = pl.ds(part * width, width)
            gate_pre = gate_pre + jnp.dot(block, gate[span, :], preferred_element_type=jnp.float32)
            up_pre = up_pre + jnp.dot(block, up[span, :], preferred_element_type=jnp.float32)
        hidden[core, at, :] = activate(gate_pre, up_pre).astype(jnp.bfloat16)
        return carry

    lax.fori_loop(0, GROUPS, first_layer, 0)
    swapped = swap(hidden, 1)
    for copy in swapped:
        copy.wait()
    arrive(3)
    down_copy = pltpu.make_async_copy(down, down_out, out_sem.at[2])
    down_copy.start()

    share = n // GROUPS
    home = me // share

    def second_layer(turn, carry):
        group = lax.rem(home + 1 + turn, GROUPS)
        at = pl.ds(pl.multiple_of(group * tile, tile), tile)
        summed = jnp.zeros((tile, width), jnp.float32)
        for part in range(cores):
            summed = summed + jnp.dot(
                hidden[part, at, :], down[pl.ds(part * columns, columns), :], preferred_element_type=jnp.float32
            )
        results[at, :] = summed.astype(jnp.bfloat16)

        def give(step, inner):
            peer = group * share + lax.rem(me + step, share)

            @pl.when(peer != me)
            def _():
                pltpu.make_async_remote_copy(
                    src_ref=results.at[pl.ds(peer * items, items)],
                    dst_ref=back.at[pl.ds(me * items, items)],
                    send_sem=send_sem.at[4],
                    recv_sem=recv_sem.at[4],
                    device_id={"fs": peer},
                    device_id_type=MESH,
                ).start()

            return inner

        lax.fori_loop(0, share, give, 0)
        return carry

    lax.fori_loop(0, GROUPS, second_layer, 0)
    kept = pltpu.make_async_copy(
        results.at[pl.ds(me * items, items)], back.at[pl.ds(me * items, items)], own_sem.at[4]
    )
    kept.start()
    kept.wait()
    gate_copy.wait()
    up_copy.wait()
    down_copy.wait()
    for phase in range(4):
        source, landing, size = phases[phase]
        drain(landing, size, send_sem.at[phase])
    drain(back, items, send_sem.at[4])
    drain(back, items, recv_sem.at[4])
    mixed = jnp.dot(mix_high[...], back[...], preferred_element_type=jnp.float32)
    mixed = mixed + jnp.dot(mix_low[...], back[...], preferred_element_type=jnp.float32)
    mixed_out[...] = mixed.astype(jnp.bfloat16)


def shards(n, cores, tokens, norm_gain, gate_weight, up_weight, down_weight, routes, route_weights):
    experts, depth, columns = gate_weight.shape
    units, width = down_weight.shape[1:]
    tok_rows, top_count = routes.shape
    items = 2 * tok_rows * top_count // experts
    total = experts * items
    gate_send = (norm_gain[None, :, None] * gate_weight).astype(jnp.bfloat16)
    up_send = (norm_gain[None, :, None] * up_weight).astype(jnp.bfloat16)
    down_send = down_weight.astype(jnp.bfloat16)

    values = tokens.astype(jnp.float32)
    squared = lax.psum(jnp.sum(values * values, axis=1), "tp")
    normed = (values * lax.rsqrt(squared / (width * cores) + epsilon)[:, None]).astype(jnp.bfloat16)

    names = jnp.arange(experts, dtype=jnp.int32)
    hits = routes[:, :, None] == names[None, None, :]
    member = jnp.any(hits, axis=1)
    weight = jnp.sum(jnp.where(hits, route_weights[:, :, None], 0.0), axis=1)
    order = jnp.arange(tok_rows, dtype=jnp.int32)
    earlier = (order[:, None] > order[None, :]).astype(jnp.bfloat16)
    place = jnp.dot(earlier, member.astype(jnp.bfloat16), preferred_element_type=jnp.float32).astype(jnp.int32)
    place = jnp.where(member, place, -1)
    slots = jnp.arange(items, dtype=jnp.int32)
    chosen = place.T[:, None, :] == slots[None, :, None]
    picks = chosen.astype(jnp.bfloat16).reshape(total, tok_rows)
    outbound = jnp.dot(picks, normed, preferred_element_type=jnp.float32).astype(jnp.bfloat16)
    rounded = lax.reduce_precision(weight, 8, 7)
    high = rounded.astype(jnp.bfloat16)
    low = (weight - rounded).astype(jnp.bfloat16)
    at_slot = place[:, :, None] == slots[None, None, :]
    zero = jnp.zeros((), jnp.bfloat16)
    mix_high = jnp.where(at_slot, high[:, :, None], zero).reshape(tok_rows, total)
    mix_low = jnp.where(at_slot, low[:, :, None], zero).reshape(tok_rows, total)

    anywhere = pl.BlockSpec(memory_space=pl.ANY)
    near = pl.BlockSpec(memory_space=pltpu.VMEM)
    mixed, gate_ready, up_ready, down_ready = pl.pallas_call(
        functools.partial(kernel, n, cores),
        out_shape=(
            jax.ShapeDtypeStruct((tok_rows, width), jnp.bfloat16),
            jax.ShapeDtypeStruct((n * depth, columns), jnp.bfloat16),
            jax.ShapeDtypeStruct((n * depth, columns), jnp.bfloat16),
            jax.ShapeDtypeStruct((n * units, width), jnp.bfloat16),
        ),
        in_specs=[anywhere] * 4 + [near] * 2,
        out_specs=(near, anywhere, anywhere, anywhere),
        scratch_shapes=[
            pltpu.VMEM((cores, total, width), jnp.bfloat16),
            pltpu.VMEM((n * depth, columns), jnp.bfloat16),
            pltpu.VMEM((n * depth, columns), jnp.bfloat16),
            pltpu.VMEM((n * units, width), jnp.bfloat16),
            pltpu.VMEM((cores, total, columns), jnp.bfloat16),
            pltpu.VMEM((total, width), jnp.bfloat16),
            pltpu.VMEM((total, width), jnp.bfloat16),
            pltpu.SemaphoreType.DMA((5,)),
            pltpu.SemaphoreType.DMA((5,)),
            pltpu.SemaphoreType.DMA((5,)),
            pltpu.SemaphoreType.DMA((3,)),
            pltpu.SemaphoreType.DMA((2, cores - 1)),
            pltpu.SemaphoreType.DMA((2, cores - 1)),
        ],
        compiler_params=pltpu.CompilerParams(
            collective_id=0, has_side_effects=True, vmem_limit_bytes=40 * 1024 * 1024
        ),
    )(outbound.reshape(experts, items, width), gate_send, up_send, down_send, mix_high, mix_low)
    return (mixed, gate_ready[None], up_ready[None], down_ready[None])


def solution(mesh):
    placed = (
        P("fs", "tp"),
        P("fs"),
        P(None, "fs", "tp"),
        P(None, "fs", "tp"),
        P(None, "fs", "tp"),
        P("fs", None),
        P("fs", None),
    )
    return jax.shard_map(
        functools.partial(shards, mesh.shape["fs"], mesh.shape["tp"]),
        mesh=mesh,
        in_specs=placed,
        out_specs=(P("fs", "tp"), P("fs", None, "tp"), P("fs", None, "tp"), P("fs", None, "tp")),
        check_vma=False,
    )
```

time: 314 us -> 270 us (0.86)
  Pallas kernels: 0 us -> 250 us
  waiting for transfers between devices: 162 us -> 0 us
  blocking collectives: 54.9 us -> 2.46 us
  starting transfers between devices: 28.6 us -> 0 us
  matrix products: 15.9 us -> 0.92 us
  between operations: 14.2 us -> 0.75 us
  local copies, waits for them, and re-layouts: 19.6 us -> 7.89 us
  other arithmetic: 16.2 us -> 8.04 us
    pallas_call x0 -> x1, Pallas kernels: none -> 250 us  [shards(): pl.pallas_call(functools.partial(kernel, n, cores), out_shape=(jax.ShapeD...]
    all_to_all x4 -> x0, waiting for transfers between devices: 161 us -> none  [the longest x1 45.3 us: shards(): lax.all_to_all(results, 'fs', split_axis=0, concat_axis=0, tiled=True)]
    all_to_all x1 -> x0, blocking collectives: 52.4 us -> none  [shards(): lax.all_to_all(up_send, 'fs', split_axis=0, concat_axis=1, tiled=True)]
    all_to_all x4 -> x0, starting transfers between devices: 28.4 us -> none  [the longest x1 7.19 us: shards(): lax.all_to_all(outbound, 'fs', split_axis=0, concat_axis=0, tiled=True)]
    dot_general x3 -> x2, matrix products: 15.9 us -> 0.92 us  [the longest x1 0.78 us: shards(): jnp.dot(picks, normed, preferred_element_type=jnp.float32)]
    scatter x1 -> x0, local copies, waits for them, and re-layouts: 7.72 us -> none  [shards(): outbound.at[slot_index].set(normed[token_index])]
    convert_element_type x3 -> x2, other arithmetic: 7.2 us -> 3.52 us  [the longest x1 3.51 us: shards(): up_send = (norm_gain[None, :, None] * up_weight).astype(jnp.bfloat16)]
    unnamed x15 -> x12, local copies, waits for them, and re-layouts: 8.51 us -> 7.22 us
  transfers between devices with their start and end apart: 6 -> 0, of which waited for: 4 -> 0; matrix products, arithmetic and copies ran while one was open for 6% -> 0% of each run, Pallas kernels for 0% -> 0%
where the time goes in v1:
time: 270 us
  Pallas kernels  250 us (93%)
  other arithmetic  8.04 us (3%)
  local copies, waits for them, and re-layouts  7.89 us (3%)
    pallas_call x1, Pallas kernels, shards(): pl.pallas_call(functools.partial(kernel, n, cores), out_shape=(jax.ShapeD...  250 us
    unnamed x12, local copies, waits for them, and re-layouts  7.22 us

profile of v1, /device:TPU:20, one launch (start us, length us, event | category | flops | bytes accessed | tf_op | source)
XLA Modules:
  0.0 269.8 jit_solution(7872871931287906179)
XLA Ops:
  0.6 1.1 fusion.1
  1.7 2.5 psum.7
  4.2 0.7 fusion.5
  4.9 0.1 fusion
  5.0 0.7 select_reduce_fusion
  5.8 0.1 eq.60
  5.8 0.2 bitcast_compare_fusion
  6.1 0.1 copy.20
  6.2 0.0 copy-start.2
  6.3 0.1 copy.21
  6.5 0.2 copy.19
  6.7 0.0 copy-start
  6.7 0.1 broadcast_select_fusion
  6.9 0.3 copy-done.2
  7.2 0.8 convolution_convert_fusion
  8.0 0.9 copy-done
  8.9 0.0 copy-start.1
  8.9 0.0 copy-start.3
  8.9 1.6 convert_element_type.46.down_in
  10.6 1.3 copy-done.1
  11.9 0.0 copy-done.3
  11.9 3.5 %multiply_convert_fusion = (bf16[16,128,512]{2,1,0:T(8,128)(2,1)S(1)}, bf16[16,128,512]{2,1,0:T(8,128)(2,1)S(1)}) fusion(f32[16,128,512]{2,1,0:T(8,128)S(1)} %copy-done.1, f32[128]{0:T(128)S(1)} %copy-done.3, f32[16,128,512]{2,1,0:T(8,128)} %param.9), kind=kLoop, calls=%fused_computation | loop fusion | flops 4194304 | bytes 12583424 | tf_op jit(solution)/shard_map/convert_element_type | solution.py:192
  15.4 249.7 %shard_map.102 = (bf16[128,1024]{1,0:T(8,128)(2,1)S(1)}, bf16[2048,512]{1,0:T(8,128)(2,1)S(1)}, bf16[2048,512]{1,0:T(8,128)(2,1)S(1)}, bf16[1024,1024]{1,0:T(8,128)(2,1)S(1)}) custom-call(bf16[16,64,1024]{2,1,0:T(8,128)(2,1)S(1)} %bitcast.12, bf16[16,128,512]{2,1,0:T(8,128)(2,1)S(1)} %get-tuple-element.17.gate_in, ...), custom_call_target="tpu_custom_call" | custom-call | tf_op jit(solution)/shard_map/pallas_call | solution.py:221
  265.1 0.7 copy.28
  265.8 1.3 copy.29
  267.1 1.3 copy.30
  268.4 1.3 copy.31
  (7 shorter events, 0.2 us)
Async XLA Ops:
  6.2 1.0 copy-start.2
  6.7 2.2 copy-start
  8.9 2.9 %copy-start.1 = (f32[16,128,512]{2,1,0:T(8,128)S(1)}, f32[16,128,512]{2,1,0:T(8,128)}, u32[]{:S(2)}) copy-start(f32[16,128,512]{2,1,0:T(8,128)} %param.10) | copy-start | bytes 12582916
  8.9 2.9 %copy-start.3 = (f32[128]{0:T(128)S(1)}, f32[128]{0:T(128)}, u32[]{:S(2)}) copy-start(f32[128]{0:T(128)} %param.8) | copy-start | bytes 1540
